TPU v7x, 256 devices: a 4x2x16 block of a 4x16x16 slice. The times are simulated.
256 devices in a mesh: grp: 2 (over y), sp: 32 (over z, core), tp: 4 (over x).
Axes of the slice: x: 4, y: 2, z: 16, core: 2. Of those that a mesh axis runs over, the one named last changes fastest.
The devices are a block of a 4x16x16 slice.
Arguments:
- hidden_in: bfloat16 [16384, 2048], P(('grp', 'sp')), parts along dimension 0, may hold values from -6 to 6
- query_latent_rows: bfloat16 [16384, 768], P(('grp', 'sp')), parts along dimension 0, may hold values from -6 to 6
- key_value_latent: bfloat16 [16384, 512], P(('grp', 'sp')), parts along dimension 0, may hold values from -6 to 6
- rotary_key: bfloat16 [16384, 32], P(('grp', 'sp')), parts along dimension 0, may hold values from -64 to 64
- query_norm_gain: float32 [768], replicated, may hold values from 0.1 to 1.9
- key_value_gain: float32 [512], replicated, may hold values from 0.1 to 1.9
- query_up_weight: bfloat16 [768, 1536], P(None, 'tp'), may hold values from -0.625 to 0.625
- key_value_up_weight: bfloat16 [512, 2048], P(None, 'tp'), may hold values from -0.25 to 0.25
- out_proj: bfloat16 [1024, 2048], P('tp'), may hold values from -0.1875 to 0.1875
- feed_gain: float32 [2048], replicated, may hold values from 0.1 to 1.9
- feed_up: bfloat16 [2048, 8192], P('sp', 'tp'), may hold values from -0.125 to 0.125
- feed_down: bfloat16 [8192, 2048], P('tp', 'sp'), may hold values from -0.0625 to 0.0625
Outputs:
- layer_out: bfloat16 [16384, 2048], P(('grp', 'sp', 'tp')), parts along dimension 0
There are 2 independent parts, one for each index of `grp`. A program takes and returns all parts, laid end to end along the dimension named above; an argument that names none is the same for every part. Nothing has to cross between parts.
All inputs are finite; a program needn't handle non-finite values.
Results may differ from a plain program's by a relative error of at most 0.02.
Values may be sent and summed in bfloat16 or wider, within the bound.
A program may use at most 128 MiB of HBM per device.

v0:
```python
import math
import jax
import jax.numpy as jnp
from jax import lax
from jax.sharding import PartitionSpec as P

QUERY_KEY_PLAIN = 64
QUERY_KEY_ROTARY = 32
VALUE_HEAD_SIZE = 64


def cut_along(value, dim, count):
    before, after = (value.shape[:dim], value.shape[dim + 1 :])
    return jnp.moveaxis(value.reshape(*before, count, -1, *after), dim, 0)


def sum_at_owner(value, axis, dim):
    count = lax.axis_size(axis)
    pieces = lax.all_to_all(cut_along(value, dim, count), axis, 0, 0, tiled=True)
    return jnp.sum(pieces.astype(jnp.float32), axis=0)


def from_everyone(value, axis):
    copies = jnp.broadcast_to(value, (lax.axis_size(axis), *value.shape))
    return lax.all_to_all(copies, axis, split_axis=0, concat_axis=0, tiled=True)


def in_order(pieces, dim):
    lengths = list(pieces.shape[1:])
    lengths[dim] *= pieces.shape[0]
    return jnp.moveaxis(pieces, 0, dim).reshape(lengths)


def gather_directly(value, axis, dim):
    pieces = from_everyone(value, axis)
    return in_order(pieces, dim)


def normalize(values, gain):
    floats = values.astype(jnp.float32)
    return floats * lax.rsqrt(jnp.mean(floats * floats, axis=-1, keepdims=True) + 1e-06) * gain


def rotate(values, position):
    half_size = values.shape[-1] // 2
    inverse = 10000.0 ** (-jnp.arange(half_size, dtype=jnp.float32) * 2.0 / values.shape[-1])
    angles = position[:, None] * inverse[None, :]
    cosine = jnp.concatenate([jnp.cos(angles), jnp.cos(angles)], axis=-1)
    sine = jnp.concatenate([jnp.sin(angles), jnp.sin(angles)], axis=-1)
    shape = (values.shape[0],) + (1,) * (values.ndim - 2) + (values.shape[-1],)
    turned = jnp.concatenate([-values[..., half_size:], values[..., :half_size]], axis=-1)
    return values * cosine.reshape(shape) + turned * sine.reshape(shape)


def on_device(
    hidden_in,
    query_latent_rows,
    key_value_latent,
    rotary_key,
    query_norm_gain,
    key_value_gain,
    query_up_weight,
    key_value_up_weight,
    out_proj,
    feed_gain,
    feed_up,
    feed_down,
):
    tokens_here = hidden_in.shape[0]
    heads_here = query_up_weight.shape[1] // (QUERY_KEY_PLAIN + QUERY_KEY_ROTARY)
    position = (lax.axis_index("sp") * tokens_here + jnp.arange(tokens_here)).astype(jnp.float32)
    scale_factor = (QUERY_KEY_PLAIN + QUERY_KEY_ROTARY) ** (-0.5)
    query_norm = normalize(query_latent_rows, query_norm_gain).astype(jnp.bfloat16)
    queries = jnp.dot(query_norm, query_up_weight, preferred_element_type=jnp.float32).reshape(
        tokens_here, heads_here, QUERY_KEY_PLAIN + QUERY_KEY_ROTARY
    )
    queries = jnp.concatenate(
        [queries[..., :QUERY_KEY_PLAIN], rotate(queries[..., QUERY_KEY_PLAIN:], position)], axis=-1
    ).astype(jnp.bfloat16)
    query_plain = queries[..., :QUERY_KEY_PLAIN]
    query_turned = queries[..., QUERY_KEY_PLAIN:]
    latent = normalize(key_value_latent, key_value_gain).astype(jnp.bfloat16)
    key_rope = rotate(rotary_key.astype(jnp.float32), position).astype(jnp.bfloat16)

    def attend_block(carry, key_plain, value_rows, rope_rows):
        row_max, denom, accum = carry
        scores = jnp.einsum(
            "qhd,khd->hqk", query_plain, key_plain, preferred_element_type=jnp.float32
        )
        scores = scores + jnp.einsum(
            "qhd,kd->hqk", query_turned, rope_rows, preferred_element_type=jnp.float32
        )
        scores = scores * scale_factor
        new_max = jnp.maximum(row_max, jnp.max(scores, axis=-1))
        expo = jnp.exp(scores - new_max[:, :, None])
        factor = jnp.exp(row_max - new_max)
        denom = denom * factor + jnp.sum(expo, axis=-1)
        update = jnp.einsum(
            "hqk,khd->qhd",
            expo.astype(jnp.bfloat16),
            value_rows,
            preferred_element_type=jnp.float32,
        )
        accum = accum * jnp.transpose(factor)[:, :, None] + update
        return (new_max, denom, accum)

    start_carry = (
        jnp.full((heads_here, tokens_here), -1e30, jnp.float32),
        jnp.zeros((heads_here, tokens_here), jnp.float32),
        jnp.zeros((tokens_here, heads_here, VALUE_HEAD_SIZE), jnp.float32),
    )
    own_keys = jnp.dot(latent, key_value_up_weight, preferred_element_type=jnp.float32).astype(
        jnp.bfloat16
    )
    pieces = (
        lax.all_gather(own_keys, "sp", axis=0, tiled=True),
        lax.all_gather(key_rope, "sp", axis=0, tiled=True),
    )
    rows_in = pieces[0].shape[0]
    block = math.gcd(rows_in, 1024)

    def step_block(index, inner):
        first = index * block
        bulk = lax.dynamic_slice_in_dim(pieces[0], first, block, 0)
        rope_rows = lax.dynamic_slice_in_dim(pieces[1], first, block, 0)
        bulk = bulk.reshape(block, heads_here, QUERY_KEY_PLAIN + VALUE_HEAD_SIZE)
        return attend_block(
            inner, bulk[..., :QUERY_KEY_PLAIN], bulk[..., QUERY_KEY_PLAIN:], rope_rows
        )

    final_carry = lax.fori_loop(0, rows_in // block, step_block, start_carry)
    denom = final_carry[1]
    accum = final_carry[2]
    mixed = (
        (accum / jnp.transpose(denom)[:, :, None])
        .astype(jnp.bfloat16)
        .reshape(tokens_here, heads_here * VALUE_HEAD_SIZE)
    )
    share = tokens_here // lax.axis_size("tp")
    lead = lax.axis_index("tp") * share
    branch = sum_at_owner(
        jnp.dot(mixed, out_proj, preferred_element_type=jnp.float32).astype(jnp.bfloat16), "tp", 0
    )
    own_rows = lax.dynamic_slice_in_dim(hidden_in, lead, share, 0)
    middle_own = (own_rows.astype(jnp.float32) + branch).astype(jnp.bfloat16)
    normed = gather_directly(normalize(middle_own, feed_gain).astype(jnp.bfloat16), "tp", 0)
    upward = jnp.dot(
        normed,
        lax.all_gather(feed_up, "sp", axis=0, tiled=True),
        preferred_element_type=jnp.float32,
    )
    activated = jnp.square(jax.nn.relu(upward)).astype(jnp.bfloat16)
    partial_sum = jnp.dot(
        activated,
        lax.all_gather(feed_down, "sp", axis=1, tiled=True),
        preferred_element_type=jnp.float32,
    )
    feed = sum_at_owner(partial_sum.astype(jnp.bfloat16), "tp", 0)
    return (middle_own.astype(jnp.float32) + feed).astype(jnp.bfloat16)


def solution(mesh):
    return jax.shard_map(
        on_device,
        mesh=mesh,
        in_specs=(
            P(("grp", "sp"), None),
            P(("grp", "sp"), None),
            P(("grp", "sp"), None),
            P(("grp", "sp"), None),
            P(),
            P(),
            P(None, "tp"),
            P(None, "tp"),
            P("tp", None),
            P(),
            P("sp", "tp"),
            P("tp", "sp"),
        ),
        out_specs=P(("grp", "sp", "tp"), None),
        check_vma=False,
    )
```

profile of v0, /device:TPU:33, one launch (start us, length us, event | category | flops | bytes accessed | tf_op | source)
XLA Modules:
  0.0 289.8 jit_solution(13299205808065012109)
XLA Ops:
  6.6 1.2 fusion.25
  7.7 2.2 convolution_convert_fusion.2
  10.1 0.7 all-gather.6.cloned.1.call-update
  10.9 0.7 all-gather.8.cloned.1.call-update
  11.6 0.7 convert_element_type.76
  12.3 0.7 slice.52
  13.0 1.2 fusion.22
  14.2 1.6 fusion.32
  16.1 55.3 %all_gather.13 = bf16[8192,32]{0,1:T(8,128)(2,1)} all-gather(bf16[256,32]{0,1:T(8,128)(2,1)S(1)} %get-tuple-element.215), channel_id=1, replica_groups=mesh['grp'=2,'sp'=32,'tp'=4] {'sp'}, dimensions={0}, use_global_device_ids=true | all-gather | bytes 540672 | tf_op jit(solution)/shard_map/all_gather | solution.py:117
  71.4 0.7 fusion.40
  72.0 30.9 %all-gather.4.cloned.1.call-done = bf16[8192,512]{1,0:T(8,128)(2,1)} async-done(((bf16[256,512]{1,0:T(8,128)(2,1)}), bf16[8192,512]{1,0:T(8,128)(2,1)}) %all-gather.4.cloned.1.call-update) | async-done | bytes 8388624 | tf_op jit(solution)/shard_map/all_gather | solution.py:116
  102.9 83.0 %while.18 = (s32[]{:T(128)}, f32[4,256]{1,0:T(4,128)S(1)}, f32[4,256]{1,0:T(4,128)S(1)}, f32[256,4,64]{0,2,1:T(8,128)S(1)}, bf16[8192,512]{1,0:T(8,128)(2,1)}, /...) while((s32[]{:T(128)}, f32[4,256]{1,0:T(4,128)S(1)}, ...), condition=%wide.region_5.0_spmd.clone, body=%wide.region_2.0_spmd.clone.sunk | while | flops 343087104 | bytes 44105964 | solution.py:131
  102.9 1.3 constant_dynamic-slice_fusion.2
  104.2 0.5 copy.26
  104.8 0.8 fusion.70
  105.6 3.5 %fusion.71 = (f32[4,256]{1,0:T(4,128)S(1)}, f32[4,256,1024]{1,2,0:T(8,128)}) fusion(bf16[256,4,32]{0,2,1:T(8,128)(2,1)S(1)} %copy-done.2, bf16[8192,32]{0,1:T(8,128)(2,1)} %get-tuple-element.307, s32[]{:T(128)S(6)} %select_n.14, f32[4,1024,256]{2,1,0:T(8,128)S(1)} %fusion.70), kind=kOutput, calls=%fused_computation.74.clone.1 | convolution fusion | flops 70253568 | bytes 8523780 | tf_op jit(solution)/shard_map/while/body/eval_jaxpr/qhd,kd->hqk/dot_general | solution.py:90
  109.1 3.1 %fusion.75 = f32[256,4,64]{0,2,1:T(8,128)S(1)} fusion(f32[4,256,1024]{1,2,0:T(8,128)} %get-tuple-element.275, f32[4,256]{1,0:T(4,128)S(1)} %get-tuple-element.302, bf16[1024,4,128]{0,2,1:T(8,128)(2,1)S(1)} %bitcast.46, f32[256,4,64]{0,2,1:T(8,128)S(1)} %get-tuple-element.292, f32[256,4]{0,1:T(4,128)S(1)} %get-tuple-element.276, pred[]{:T(512)S(6)} %compare.3), kind=kOutput, calls=%fused_computation.8.clone.1 | convolution fusion | flops 136511488 | bytes 5251073 | tf_op jit(solution)/shard_map/while/body/eval_jaxpr/hqk,khd->qhd/dot_general | solution.py:98
  112.6 0.6 fusion.73
  113.2 1.3 constant_dynamic-slice_fusion.2
  114.5 0.5 copy.26
  115.0 0.8 fusion.70
  115.9 3.5 %fusion.71 = (f32[4,256]{1,0:T(4,128)S(1)}, f32[4,256,1024]{1,2,0:T(8,128)}) fusion(bf16[256,4,32]{0,2,1:T(8,128)(2,1)S(1)} %copy-done.2, bf16[8192,32]{0,1:T(8,128)(2,1)} %get-tuple-element.307, s32[]{:T(128)S(6)} %select_n.14, f32[4,1024,256]{2,1,0:T(8,128)S(1)} %fusion.70), kind=kOutput, calls=%fused_computation.74.clone.1 | convolution fusion | flops 70253568 | bytes 8523780 | tf_op jit(solution)/shard_map/while/body/eval_jaxpr/qhd,kd->hqk/dot_general | solution.py:90
  119.4 3.2 %fusion.75 = f32[256,4,64]{0,2,1:T(8,128)S(1)} fusion(f32[4,256,1024]{1,2,0:T(8,128)} %get-tuple-element.275, f32[4,256]{1,0:T(4,128)S(1)} %get-tuple-element.302, bf16[1024,4,128]{0,2,1:T(8,128)(2,1)S(1)} %bitcast.46, f32[256,4,64]{0,2,1:T(8,128)S(1)} %get-tuple-element.292, f32[256,4]{0,1:T(4,128)S(1)} %get-tuple-element.276, pred[]{:T(512)S(6)} %compare.3), kind=kOutput, calls=%fused_computation.8.clone.1 | convolution fusion | flops 136511488 | bytes 5251073 | tf_op jit(solution)/shard_map/while/body/eval_jaxpr/hqk,khd->qhd/dot_general | solution.py:98
  123.0 0.6 fusion.73
  123.6 1.3 constant_dynamic-slice_fusion.2
  125.5 0.8 fusion.70
  126.3 3.5 %fusion.71 = (f32[4,256]{1,0:T(4,128)S(1)}, f32[4,256,1024]{1,2,0:T(8,128)}) fusion(bf16[256,4,32]{0,2,1:T(8,128)(2,1)S(1)} %copy-done.2, bf16[8192,32]{0,1:T(8,128)(2,1)} %get-tuple-element.307, s32[]{:T(128)S(6)} %select_n.14, f32[4,1024,256]{2,1,0:T(8,128)S(1)} %fusion.70), kind=kOutput, calls=%fused_computation.74.clone.1 | convolution fusion | flops 70253568 | bytes 8523780 | tf_op jit(solution)/shard_map/while/body/eval_jaxpr/qhd,kd->hqk/dot_general | solution.py:90
  129.8 3.2 %fusion.75 = f32[256,4,64]{0,2,1:T(8,128)S(1)} fusion(f32[4,256,1024]{1,2,0:T(8,128)} %get-tuple-element.275, f32[4,256]{1,0:T(4,128)S(1)} %get-tuple-element.302, bf16[1024,4,128]{0,2,1:T(8,128)(2,1)S(1)} %bitcast.46, f32[256,4,64]{0,2,1:T(8,128)S(1)} %get-tuple-element.292, f32[256,4]{0,1:T(4,128)S(1)} %get-tuple-element.276, pred[]{:T(512)S(6)} %compare.3), kind=kOutput, calls=%fused_computation.8.clone.1 | convolution fusion | flops 136511488 | bytes 5251073 | tf_op jit(solution)/shard_map/while/body/eval_jaxpr/hqk,khd->qhd/dot_general | solution.py:98
  133.4 0.6 fusion.73
  134.0 1.3 constant_dynamic-slice_fusion.2
  135.9 0.8 fusion.70
  136.7 3.5 %fusion.71 = (f32[4,256]{1,0:T(4,128)S(1)}, f32[4,256,1024]{1,2,0:T(8,128)}) fusion(bf16[256,4,32]{0,2,1:T(8,128)(2,1)S(1)} %copy-done.2, bf16[8192,32]{0,1:T(8,128)(2,1)} %get-tuple-element.307, s32[]{:T(128)S(6)} %select_n.14, f32[4,1024,256]{2,1,0:T(8,128)S(1)} %fusion.70), kind=kOutput, calls=%fused_computation.74.clone.1 | convolution fusion | flops 70253568 | bytes 8523780 | tf_op jit(solution)/shard_map/while/body/eval_jaxpr/qhd,kd->hqk/dot_general | solution.py:90
  140.3 3.2 %fusion.75 = f32[256,4,64]{0,2,1:T(8,128)S(1)} fusion(f32[4,256,1024]{1,2,0:T(8,128)} %get-tuple-element.275, f32[4,256]{1,0:T(4,128)S(1)} %get-tuple-element.302, bf16[1024,4,128]{0,2,1:T(8,128)(2,1)S(1)} %bitcast.46, f32[256,4,64]{0,2,1:T(8,128)S(1)} %get-tuple-element.292, f32[256,4]{0,1:T(4,128)S(1)} %get-tuple-element.276, pred[]{:T(512)S(6)} %compare.3), kind=kOutput, calls=%fused_computation.8.clone.1 | convolution fusion | flops 136511488 | bytes 5251073 | tf_op jit(solution)/shard_map/while/body/eval_jaxpr/hqk,khd->qhd/dot_general | solution.py:98
  143.8 0.6 fusion.73
  144.5 1.3 constant_dynamic-slice_fusion.2
  146.4 0.8 fusion.70
  147.2 3.5 %fusion.71 = (f32[4,256]{1,0:T(4,128)S(1)}, f32[4,256,1024]{1,2,0:T(8,128)}) fusion(bf16[256,4,32]{0,2,1:T(8,128)(2,1)S(1)} %copy-done.2, bf16[8192,32]{0,1:T(8,128)(2,1)} %get-tuple-element.307, s32[]{:T(128)S(6)} %select_n.14, f32[4,1024,256]{2,1,0:T(8,128)S(1)} %fusion.70), kind=kOutput, calls=%fused_computation.74.clone.1 | convolution fusion | flops 70253568 | bytes 8523780 | tf_op jit(solution)/shard_map/while/body/eval_jaxpr/qhd,kd->hqk/dot_general | solution.py:90
  150.7 3.2 %fusion.75 = f32[256,4,64]{0,2,1:T(8,128)S(1)} fusion(f32[4,256,1024]{1,2,0:T(8,128)} %get-tuple-element.275, f32[4,256]{1,0:T(4,128)S(1)} %get-tuple-element.302, bf16[1024,4,128]{0,2,1:T(8,128)(2,1)S(1)} %bitcast.46, f32[256,4,64]{0,2,1:T(8,128)S(1)} %get-tuple-element.292, f32[256,4]{0,1:T(4,128)S(1)} %get-tuple-element.276, pred[]{:T(512)S(6)} %compare.3), kind=kOutput, calls=%fused_computation.8.clone.1 | convolution fusion | flops 136511488 | bytes 5251073 | tf_op jit(solution)/shard_map/while/body/eval_jaxpr/hqk,khd->qhd/dot_general | solution.py:98
  154.3 0.6 fusion.73
  154.9 1.3 constant_dynamic-slice_fusion.2
  156.8 0.8 fusion.70
  157.6 3.5 %fusion.71 = (f32[4,256]{1,0:T(4,128)S(1)}, f32[4,256,1024]{1,2,0:T(8,128)}) fusion(bf16[256,4,32]{0,2,1:T(8,128)(2,1)S(1)} %copy-done.2, bf16[8192,32]{0,1:T(8,128)(2,1)} %get-tuple-element.307, s32[]{:T(128)S(6)} %select_n.14, f32[4,1024,256]{2,1,0:T(8,128)S(1)} %fusion.70), kind=kOutput, calls=%fused_computation.74.clone.1 | convolution fusion | flops 70253568 | bytes 8523780 | tf_op jit(solution)/shard_map/while/body/eval_jaxpr/qhd,kd->hqk/dot_general | solution.py:90
  161.2 3.2 %fusion.75 = f32[256,4,64]{0,2,1:T(8,128)S(1)} fusion(f32[4,256,1024]{1,2,0:T(8,128)} %get-tuple-element.275, f32[4,256]{1,0:T(4,128)S(1)} %get-tuple-element.302, bf16[1024,4,128]{0,2,1:T(8,128)(2,1)S(1)} %bitcast.46, f32[256,4,64]{0,2,1:T(8,128)S(1)} %get-tuple-element.292, f32[256,4]{0,1:T(4,128)S(1)} %get-tuple-element.276, pred[]{:T(512)S(6)} %compare.3), kind=kOutput, calls=%fused_computation.8.clone.1 | convolution fusion | flops 136511488 | bytes 5251073 | tf_op jit(solution)/shard_map/while/body/eval_jaxpr/hqk,khd->qhd/dot_general | solution.py:98
  164.7 0.6 fusion.73
  165.4 1.3 constant_dynamic-slice_fusion.2
  167.2 0.8 fusion.70
  168.0 3.5 %fusion.71 = (f32[4,256]{1,0:T(4,128)S(1)}, f32[4,256,1024]{1,2,0:T(8,128)}) fusion(bf16[256,4,32]{0,2,1:T(8,128)(2,1)S(1)} %copy-done.2, bf16[8192,32]{0,1:T(8,128)(2,1)} %get-tuple-element.307, s32[]{:T(128)S(6)} %select_n.14, f32[4,1024,256]{2,1,0:T(8,128)S(1)} %fusion.70), kind=kOutput, calls=%fused_computation.74.clone.1 | convolution fusion | flops 70253568 | bytes 8523780 | tf_op jit(solution)/shard_map/while/body/eval_jaxpr/qhd,kd->hqk/dot_general | solution.py:90
  171.6 3.1 %fusion.75 = f32[256,4,64]{0,2,1:T(8,128)S(1)} fusion(f32[4,256,1024]{1,2,0:T(8,128)} %get-tuple-element.275, f32[4,256]{1,0:T(4,128)S(1)} %get-tuple-element.302, bf16[1024,4,128]{0,2,1:T(8,128)(2,1)S(1)} %bitcast.46, f32[256,4,64]{0,2,1:T(8,128)S(1)} %get-tuple-element.292, f32[256,4]{0,1:T(4,128)S(1)} %get-tuple-element.276, pred[]{:T(512)S(6)} %compare.3), kind=kOutput, calls=%fused_computation.8.clone.1 | convolution fusion | flops 136511488 | bytes 5251073 | tf_op jit(solution)/shard_map/while/body/eval_jaxpr/hqk,khd->qhd/dot_general | solution.py:98
  175.0 0.6 fusion.73
  175.6 1.3 constant_dynamic-slice_fusion.2
  177.5 0.8 fusion.70
  178.3 3.5 %fusion.71 = (f32[4,256]{1,0:T(4,128)S(1)}, f32[4,256,1024]{1,2,0:T(8,128)}) fusion(bf16[256,4,32]{0,2,1:T(8,128)(2,1)S(1)} %copy-done.2, bf16[8192,32]{0,1:T(8,128)(2,1)} %get-tuple-element.307, s32[]{:T(128)S(6)} %select_n.14, f32[4,1024,256]{2,1,0:T(8,128)S(1)} %fusion.70), kind=kOutput, calls=%fused_computation.74.clone.1 | convolution fusion | flops 70253568 | bytes 8523780 | tf_op jit(solution)/shard_map/while/body/eval_jaxpr/qhd,kd->hqk/dot_general | solution.py:90
  181.8 3.1 %fusion.75 = f32[256,4,64]{0,2,1:T(8,128)S(1)} fusion(f32[4,256,1024]{1,2,0:T(8,128)} %get-tuple-element.275, f32[4,256]{1,0:T(4,128)S(1)} %get-tuple-element.302, bf16[1024,4,128]{0,2,1:T(8,128)(2,1)S(1)} %bitcast.46, f32[256,4,64]{0,2,1:T(8,128)S(1)} %get-tuple-element.292, f32[256,4]{0,1:T(4,128)S(1)} %get-tuple-element.276, pred[]{:T(512)S(6)} %compare.3), kind=kOutput, calls=%fused_computation.8.clone.1 | convolution fusion | flops 136511488 | bytes 5251073 | tf_op jit(solution)/shard_map/while/body/eval_jaxpr/hqk,khd->qhd/dot_general | solution.py:98
  185.3 0.6 fusion.73
  185.9 1.4 convolution_convert_fusion
  187.4 4.2 %all-to-all-start = ((bf16[4,64,2048]{2,1,0:T(8,128)(2,1)}), bf16[4,64,2048]{2,1,0:T(8,128)(2,1)S(1)}, u32[]{:S(2)}, u32[]{:S(2)}) async-start(bf16[4,64,2048]{2,1,0:T(8,128)(2,1)} %bitcast.3), calls=%async_computation | async-start | bytes 2097152 | tf_op jit(solution)/shard_map/all_to_all | solution.py:19
  191.5 14.8 %all-to-all-done = bf16[4,64,2048]{2,1,0:T(8,128)(2,1)S(1)} async-done(((bf16[4,64,2048]{2,1,0:T(8,128)(2,1)}), bf16[4,64,2048]{2,1,0:T(8,128)(2,1)S(1)}, u32[]{:S(2)}, u32[]{:S(2)}) %all-to-all-start) | async-done | bytes 1048608 | tf_op jit(solution)/shard_map/all_to_all | solution.py:19
  206.5 1.1 fusion.28
  207.8 1.1 broadcast_in_dim.17
  208.9 3.6 %all-to-all-start.1 = ((bf16[4,64,2048]{2,1,0:T(8,128)(2,1)}), bf16[4,64,2048]{2,1,0:T(8,128)(2,1)S(1)}, u32[]{:S(2)}, u32[]{:S(2)}) async-start(bf16[4,64,2048]{2,1,0:T(8,128)(2,1)} %broadcast_in_dim.17), calls=%async_computation.1 | async-start | bytes 2097152 | tf_op jit(solution)/shard_map/all_to_all | solution.py:25
  212.5 41.0 %all-gather.8.cloned.1.call-done = bf16[2048,2048]{0,1:T(8,128)(2,1)} async-done(((bf16[2048,64]{0,1:T(8,128)(2,1)}), bf16[2048,2048]{0,1:T(8,128)(2,1)}) %all-gather.8.cloned.1.call-update) | async-done | bytes 8388624 | tf_op jit(solution)/shard_map/all_gather | solution.py:155
  253.6 10.3 %convolution_convert_fusion.1 = bf16[256,2048]{1,0:T(8,128)(2,1)S(1)} fusion(bf16[2048,2048]{0,1:T(8,128)(2,1)} %all-gather.8.cloned.1.call-done, bf16[256,2048]{1,0:T(8,128)(2,1)S(1)} %bitcast.50, bf16[2048,2048]{1,0:T(8,128)(2,1)} %all-gather.6.cloned.1.call-done), kind=kOutput, calls=%fused_computation.26 | convolution fusion | flops 4297064448 | bytes 18874368 | tf_op jit(solution)/shard_map/dot_general | solution.py:153
  263.8 18.5 %all_to_all.15 = bf16[4,64,2048]{2,1,0:T(8,128)(2,1)S(1)} all-to-all(bf16[4,64,2048]{2,1,0:T(8,128)(2,1)S(1)} %bitcast.51), channel_id=1, replica_groups=mesh['grp'=2,'sp'=32,'tp'=4] {'tp'}, dimensions={0} | all-to-all | bytes 2097152 | tf_op jit(solution)/shard_map/all_to_all | solution.py:19
  282.5 0.8 fusion.31
  (90 shorter events, 7.6 us)
Async XLA Ops:
  6.5 179.4 %copy-start = (bf16[256,2048]{1,0:T(8,128)(2,1)S(1)}, bf16[256,2048]{1,0:T(8,128)(2,1)}, u32[]{:S(2)}) copy-start(bf16[256,2048]{1,0:T(8,128)(2,1)} %param.22) | copy-start | bytes 3145732
  6.6 9.5 %copy-start.3 = (bf16[256,32]{0,1:T(8,128)(2,1)S(1)}, bf16[256,32]{0,1:T(8,128)(2,1)}, u32[]{:S(2)}) copy-start(bf16[256,32]{0,1:T(8,128)(2,1)} %param.17) | copy-start | bytes 49156
  6.6 96.4 %all-gather.4.cloned.1.call-start = ((), (), s32[]{:S(2)}) async-start(), calls=%async_computation.3 | async-start | bytes 8650752 | tf_op jit(solution)/shard_map/all_gather | solution.py:116
  10.0 202.5 %all-gather.6.cloned.1.call-start = ((), (), s32[]{:S(2)}) async-start(), calls=%async_computation.4 | async-start | bytes 8650752 | tf_op jit(solution)/shard_map/all_gather | solution.py:149
  10.8 242.7 %all-gather.8.cloned.1.call-start = ((), (), s32[]{:S(2)}) async-start(), calls=%async_computation.5 | async-start | bytes 8650752 | tf_op jit(solution)/shard_map/all_gather | solution.py:155
  104.8 0.8 copy-start.2
  109.1 3.4 %copy-start.1 = (f32[4,256,1024]{1,2,0:T(8,128)S(1)}, f32[4,256,1024]{1,2,0:T(8,128)}, u32[]{:S(2)}) copy-start(f32[4,256,1024]{1,2,0:T(8,128)} %get-tuple-element.275) | copy-start | bytes 12582916 | tf_op jit(solution)/shard_map/while
  115.0 0.8 copy-start.2
  119.4 3.6 %copy-start.1 = (f32[4,256,1024]{1,2,0:T(8,128)S(1)}, f32[4,256,1024]{1,2,0:T(8,128)}, u32[]{:S(2)}) copy-start(f32[4,256,1024]{1,2,0:T(8,128)} %get-tuple-element.275) | copy-start | bytes 12582916 | tf_op jit(solution)/shard_map/while
  125.5 0.8 copy-start.2
  129.8 3.6 %copy-start.1 = (f32[4,256,1024]{1,2,0:T(8,128)S(1)}, f32[4,256,1024]{1,2,0:T(8,128)}, u32[]{:S(2)}) copy-start(f32[4,256,1024]{1,2,0:T(8,128)} %get-tuple-element.275) | copy-start | bytes 12582916 | tf_op jit(solution)/shard_map/while
  135.9 0.8 copy-start.2
  140.3 3.6 %copy-start.1 = (f32[4,256,1024]{1,2,0:T(8,128)S(1)}, f32[4,256,1024]{1,2,0:T(8,128)}, u32[]{:S(2)}) copy-start(f32[4,256,1024]{1,2,0:T(8,128)} %get-tuple-element.275) | copy-start | bytes 12582916 | tf_op jit(solution)/shard_map/while
  146.3 0.8 copy-start.2
  150.7 3.6 %copy-start.1 = (f32[4,256,1024]{1,2,0:T(8,128)S(1)}, f32[4,256,1024]{1,2,0:T(8,128)}, u32[]{:S(2)}) copy-start(f32[4,256,1024]{1,2,0:T(8,128)} %get-tuple-element.275) | copy-start | bytes 12582916 | tf_op jit(solution)/shard_map/while
  156.8 0.8 copy-start.2
  161.2 3.6 %copy-start.1 = (f32[4,256,1024]{1,2,0:T(8,128)S(1)}, f32[4,256,1024]{1,2,0:T(8,128)}, u32[]{:S(2)}) copy-start(f32[4,256,1024]{1,2,0:T(8,128)} %get-tuple-element.275) | copy-start | bytes 12582916 | tf_op jit(solution)/shard_map/while
  167.2 0.8 copy-start.2
  171.6 3.4 %copy-start.1 = (f32[4,256,1024]{1,2,0:T(8,128)S(1)}, f32[4,256,1024]{1,2,0:T(8,128)}, u32[]{:S(2)}) copy-start(f32[4,256,1024]{1,2,0:T(8,128)} %get-tuple-element.275) | copy-start | bytes 12582916 | tf_op jit(solution)/shard_map/while
  177.5 0.8 copy-start.2
  181.8 3.4 %copy-start.1 = (f32[4,256,1024]{1,2,0:T(8,128)S(1)}, f32[4,256,1024]{1,2,0:T(8,128)}, u32[]{:S(2)}) copy-start(f32[4,256,1024]{1,2,0:T(8,128)} %get-tuple-element.275) | copy-start | bytes 12582916 | tf_op jit(solution)/shard_map/while
  185.9 21.7 %copy-start.4 = (f32[2048]{0:T(1024)S(1)}, f32[2048]{0:T(1024)}, u32[]{:S(2)}) copy-start(f32[2048]{0:T(1024)} %param.23) | copy-start | bytes 24580
  187.4 18.9 %all-to-all-start = ((bf16[4,64,2048]{2,1,0:T(8,128)(2,1)}), bf16[4,64,2048]{2,1,0:T(8,128)(2,1)S(1)}, u32[]{:S(2)}, u32[]{:S(2)}) async-start(bf16[4,64,2048]{2,1,0:T(8,128)(2,1)} %bitcast.3), calls=%async_computation | async-start | bytes 2097152 | tf_op jit(solution)/shard_map/all_to_all | solution.py:19
  208.9 44.7 %all-to-all-start.1 = ((bf16[4,64,2048]{2,1,0:T(8,128)(2,1)}), bf16[4,64,2048]{2,1,0:T(8,128)(2,1)S(1)}, u32[]{:S(2)}, u32[]{:S(2)}) async-start(bf16[4,64,2048]{2,1,0:T(8,128)(2,1)} %broadcast_in_dim.17), calls=%async_computation.1 | async-start | bytes 2097152 | tf_op jit(solution)/shard_map/all_to_all | solution.py:25
Sparse Core Ops, SparseCore 0:
  10.1 92.7 all-gather.3
  104.8 73.3 all-gather.5
  180.1 73.4 all-gather.7
where the time goes:
time: 291 us; the launch traced here: 290 us
  waiting for transfers between devices  88.2 us (30%)
  matrix products  75.2 us (26%)
  blocking collectives  73.7 us (25%)
  local copies, waits for them, and re-layouts  19.8 us (7%)
  between operations  13.3 us (5%)
  other arithmetic  11.1 us (4%)
  starting transfers between devices  7.9 us (3%)
    all_gather x1, blocking collectives, on_device(): lax.all_gather(key_rope, 'sp', axis=0, tiled=True)  55.3 us
    all_gather x1, waiting for transfers between devices, on_device(): lax.all_gather(feed_down, 'sp', axis=1, tiled=True)  41 us
    all_gather x1, waiting for transfers between devices, on_device(): lax.all_gather(own_keys, 'sp', axis=0, tiled=True)  30.9 us
    dot_general x8, matrix products, attend_block(): jnp.einsum('qhd,kd->hqk', query_turned, rope_rows, preferred_element_type...  28.1 us
    dot_general x8, matrix products, attend_block(): jnp.einsum('hqk,khd->qhd', expo.astype(jnp.bfloat16), value_rows, preferr...  25.4 us
    all_to_all x1, blocking collectives, sum_at_owner(): lax.all_to_all(cut_along(value, dim, count), axis, 0, 0, tiled=True)  18.5 us
    all_to_all x1, waiting for transfers between devices, sum_at_owner(): lax.all_to_all(cut_along(value, dim, count), axis, 0, 0, tiled=True)  14.8 us
    dynamic_slice x16, local copies, waits for them, and re-layouts, step_block(): bulk = lax.dynamic_slice_in_dim(pieces[0], first, block, 0)  14.7 us
  transfers between devices with their start and end apart: 5, of which 3 were waited for; matrix products, arithmetic and copies ran while one was open for 30% of the time, Pallas kernels for 0%

commit v1 on v0

--- a/solution.py
+++ b/solution.py
@@ -7,6 +7,14 @@
 QUERY_KEY_PLAIN = 64
 QUERY_KEY_ROTARY = 32
 VALUE_HEAD_SIZE = 64
+
+
+def tiled_gather(value, axis, dim):
+    size = lax.axis_size(axis)
+    repeats = [size if d == dim else 1 for d in range(value.ndim)]
+    return lax.all_to_all(
+        jnp.tile(value, repeats), axis, split_axis=dim, concat_axis=dim, tiled=True
+    )
 
 
 def cut_along(value, dim, count):
@@ -112,10 +120,7 @@
     own_keys = jnp.dot(latent, key_value_up_weight, preferred_element_type=jnp.float32).astype(
         jnp.bfloat16
     )
-    pieces = (
-        lax.all_gather(own_keys, "sp", axis=0, tiled=True),
-        lax.all_gather(key_rope, "sp", axis=0, tiled=True),
-    )
+    pieces = (tiled_gather(own_keys, "sp", 0), lax.all_gather(key_rope, "sp", axis=0, tiled=True))
     rows_in = pieces[0].shape[0]
     block = math.gcd(rows_in, 1024)
 

time: 291 us -> 673 us (2.31)
  blocking collectives: 73.7 us -> 474 us
  waiting for transfers between devices: 88.2 us -> 29.8 us
  starting transfers between devices: 7.9 us -> 33.8 us
  local copies, waits for them, and re-layouts: 19.8 us -> 35 us
    all_gather x1, blocking collectives: 55.3 us -> 459 us  [on_device(): lax.all_gather(key_rope, 'sp', axis=0, tiled=True)]
    all_gather x1, waiting for transfers between devices: 41 us -> 0.02 us  [on_device(): lax.all_gather(feed_down, 'sp', axis=1, tiled=True)]
    all_gather x1 -> x0, waiting for transfers between devices: 30.9 us -> none  [on_device(): lax.all_gather(own_keys, 'sp', axis=0, tiled=True)]
    all_to_all x0 -> x1, starting transfers between devices: none -> 25.6 us  [tiled_gather(): lax.all_to_all(jnp.tile(value, repeats), axis, split_axis=dim, concat_axi...]
    all_to_all x1, waiting for transfers between devices: 0.01 us -> 13.6 us  [from_everyone(): return lax.all_to_all(copies, axis, split_axis=0, concat_axis=0, tiled=True)]
    all_to_all x0 -> x1, local copies, waits for them, and re-layouts: none -> 12 us  [tiled_gather(): lax.all_to_all(jnp.tile(value, repeats), axis, split_axis=dim, concat_axi...]
  transfers between devices with their start and end apart: 5 -> 5, of which waited for: 3 -> 2; matrix products, arithmetic and copies ran while one was open for 30% -> 14% of each run, Pallas kernels for 0% -> 0%
where the time goes in v1:
time: 673 us; the launch traced here: 669 us
  blocking collectives  474 us (70%)
  matrix products  73.2 us (11%)
  local copies, waits for them, and re-layouts  35 us (5%)
  starting transfers between devices  33.8 us (5%)
  waiting for transfers between devices  29.8 us (4%)
  between operations  13.7 us (2%)
  other arithmetic  9.34 us (1%)
    all_gather x1, blocking collectives, on_device(): lax.all_gather(key_rope, 'sp', axis=0, tiled=True)  459 us
    dot_general x8, matrix products, attend_block(): jnp.einsum('qhd,kd->hqk', query_turned, rope_rows, preferred_element_type...  28.3 us
    all_to_all x1, starting transfers between devices, tiled_gather(): lax.all_to_all(jnp.tile(value, repeats), axis, split_axis=dim, concat_axi...  25.6 us
    dot_general x8, matrix products, attend_block(): jnp.einsum('hqk,khd->qhd', expo.astype(jnp.bfloat16), value_rows, preferr...  25.1 us
    all_to_all x1, blocking collectives, sum_at_owner(): lax.all_to_all(cut_along(value, dim, count), axis, 0, 0, tiled=True)  15.2 us
    all_to_all x1, waiting for transfers between devices, sum_at_owner(): lax.all_to_all(cut_along(value, dim, count), axis, 0, 0, tiled=True)  14.8 us
    dynamic_slice x16, local copies, waits for them, and re-layouts, step_block(): bulk = lax.dynamic_slice_in_dim(pieces[0], first, block, 0)  14.7 us
    all_to_all x1, waiting for transfers between devices, from_everyone(): return lax.all_to_all(copies, axis, split_axis=0, concat_axis=0, tiled=True)  13.6 us
  transfers between devices with their start and end apart: 5, of which 2 were waited for; matrix products, arithmetic and copies ran while one was open for 14% of the time, Pallas kernels for 0%

profile of v1, /device:TPU:33, one launch (start us, length us, event | category | flops | bytes accessed | tf_op | source)
XLA Modules:
  0.0 669.4 jit_solution(5713428881621603947)
XLA Ops:
  6.6 1.2 fusion.25
  7.7 1.5 convolution_convert_fusion.2
  9.4 4.2 tile.2
  13.5 25.6 %all-to-all-start = ((bf16[32,256,512]{1,2,0:T(8,128)(2,1)}), bf16[32,256,512]{1,2,0:T(8,128)(2,1)}, u32[]{:S(2)}, u32[]{:S(2)}) async-start(bf16[32,256,512]{1,2,0:T(8,128)(2,1)} %tile.2), calls=%async_computation | async-start | bytes 16777216 | tf_op jit(solution)/shard_map/all_to_all | solution.py:15
  39.2 0.7 all-gather.3.cloned.1.call-update
  40.0 0.7 all-gather.5.cloned.1.call-update
  41.7 0.7 fusion.40
  42.4 458.9 %all_gather.9 = bf16[8192,32]{0,1:T(8,128)(2,1)} all-gather(bf16[256,32]{0,1:T(8,128)(2,1)S(1)} %get-tuple-element.207), channel_id=1, replica_groups=mesh['grp'=2,'sp'=32,'tp'=4] {'sp'}, dimensions={0}, use_global_device_ids=true | all-gather | bytes 540672 | tf_op jit(solution)/shard_map/all_gather | solution.py:123
  501.3 12.0 %copy.27 = bf16[32,256,512]{2,1,0:T(8,128)(2,1)} copy(bf16[32,256,512]{1,2,0:T(8,128)(2,1)} %all-to-all-done) | data formatting | bytes 16777216 | tf_op jit(solution)/shard_map/all_to_all | solution.py:15
  513.3 82.4 %while.18 = (s32[]{:T(128)}, f32[4,256]{1,0:T(4,128)S(1)}, f32[4,256]{1,0:T(4,128)S(1)}, f32[256,4,64]{0,2,1:T(8,128)S(1)}, bf16[8192,512]{1,0:T(8,128)(2,1)}, /...) while((s32[]{:T(128)}, f32[4,256]{1,0:T(4,128)S(1)}, ...), condition=%wide.region_5.0_spmd.clone, body=%wide.region_2.0_spmd.clone.sunk | while | flops 343087104 | bytes 44105964 | solution.py:136
  513.3 1.3 constant_dynamic-slice_fusion.2
  514.6 0.5 copy.34
  515.1 0.8 fusion.70
  516.0 3.5 fusion.71
  519.5 3.1 fusion.75
  523.0 0.6 fusion.73
  523.6 1.3 constant_dynamic-slice_fusion.2
  524.9 0.5 copy.34
  525.4 0.8 fusion.70
  526.3 3.5 fusion.71
  529.8 3.1 fusion.75
  533.3 0.6 fusion.73
  533.9 1.3 constant_dynamic-slice_fusion.2
  535.2 0.5 copy.34
  535.7 0.8 fusion.70
  536.6 3.5 fusion.71
  540.1 3.1 fusion.75
  543.6 0.6 fusion.73
  544.2 1.3 constant_dynamic-slice_fusion.2
  545.5 0.5 copy.34
  546.0 0.8 fusion.70
  546.9 3.5 fusion.71
  550.4 3.1 fusion.75
  553.9 0.6 fusion.73
  554.5 1.3 constant_dynamic-slice_fusion.2
  556.3 0.8 fusion.70
  557.2 3.5 fusion.71
  560.7 3.1 fusion.75
  564.2 0.6 fusion.73
  564.8 1.3 constant_dynamic-slice_fusion.2
  566.6 0.8 fusion.70
  567.5 3.5 fusion.71
  571.0 3.1 fusion.75
  574.5 0.6 fusion.73
  575.1 1.3 constant_dynamic-slice_fusion.2
  576.9 0.8 fusion.70
  577.8 3.5 fusion.71
  581.3 3.1 fusion.75
  584.8 0.6 fusion.73
  585.4 1.3 constant_dynamic-slice_fusion.2
  587.2 0.8 fusion.70
  588.1 3.5 fusion.71
  591.6 3.1 fusion.75
  595.0 0.6 fusion.73
  595.7 1.4 convolution_convert_fusion
  597.2 4.2 all-to-all-start.1
  601.4 14.8 %all-to-all-done.1 = bf16[4,64,2048]{2,1,0:T(8,128)(2,1)S(1)} async-done(((bf16[4,64,2048]{2,1,0:T(8,128)(2,1)}), bf16[4,64,2048]{2,1,0:T(8,128)(2,1)S(1)}, u32[]{:S(2)}, u32[]{:S(2)}) %all-to-all-start.1) | async-done | bytes 1048608 | tf_op jit(solution)/shard_map/all_to_all | solution.py:27
  616.3 1.1 fusion.28
  617.6 1.1 broadcast_in_dim.17
  618.7 3.8 all-to-all-start.2
  622.6 13.6 %all-to-all-done.2 = bf16[4,64,2048]{2,1,0:T(8,128)(2,1)S(1)} async-done(((bf16[4,64,2048]{2,1,0:T(8,128)(2,1)}), bf16[4,64,2048]{2,1,0:T(8,128)(2,1)S(1)}, u32[]{:S(2)}, u32[]{:S(2)}) %all-to-all-start.2) | async-done | bytes 1048608 | tf_op jit(solution)/shard_map/all_to_all | solution.py:33
  636.1 10.3 %convolution_convert_fusion.1 = bf16[256,2048]{1,0:T(8,128)(2,1)S(1)} fusion(bf16[2048,2048]{0,1:T(8,128)(2,1)} %all-gather.5.cloned.1.call-done, bf16[256,2048]{1,0:T(8,128)(2,1)S(1)} %bitcast.52, bf16[2048,2048]{1,0:T(8,128)(2,1)} %all-gather.3.cloned.1.call-done), kind=kOutput, calls=%fused_computation.26 | convolution fusion | flops 4297064448 | bytes 18874368 | tf_op jit(solution)/shard_map/dot_general | solution.py:158
  646.4 15.2 %all_to_all.24 = bf16[4,64,2048]{2,1,0:T(8,128)(2,1)S(1)} all-to-all(bf16[4,64,2048]{2,1,0:T(8,128)(2,1)S(1)} %bitcast.53), channel_id=1, replica_groups=mesh['grp'=2,'sp'=32,'tp'=4] {'tp'}, dimensions={0} | all-to-all | bytes 2097152 | tf_op jit(solution)/shard_map/all_to_all | solution.py:27
  661.8 0.8 fusion.31
  (98 shorter events, 6.9 us)
Async XLA Ops:
  6.5 589.2 %copy-start = (bf16[256,2048]{1,0:T(8,128)(2,1)S(1)}, bf16[256,2048]{1,0:T(8,128)(2,1)}, u32[]{:S(2)}) copy-start(bf16[256,2048]{1,0:T(8,128)(2,1)} %param.22) | copy-start | bytes 3145732
  13.5 27.2 %copy-start.5 = (bf16[256,32]{0,1:T(8,128)(2,1)S(1)}, bf16[256,32]{0,1:T(8,128)(2,1)}, u32[]{:S(2)}) copy-start(bf16[256,32]{0,1:T(8,128)(2,1)} %param.17) | copy-start | bytes 49156
  13.5 27.3 %copy-start.3 = (bf16[256,768]{1,0:T(8,128)(2,1)S(1)}, bf16[256,768]{1,0:T(8,128)(2,1)}, u32[]{:S(2)}) copy-start(bf16[256,768]{1,0:T(8,128)(2,1)} %param.15) | copy-start | bytes 1179652
  13.5 27.5 %copy-start.4 = (bf16[768,384]{1,0:T(8,128)(2,1)S(1)}, bf16[768,384]{1,0:T(8,128)(2,1)}, u32[]{:S(2)}) copy-start(bf16[768,384]{1,0:T(8,128)(2,1)} %param.20) | copy-start | bytes 1769476
  13.5 27.5 %copy-start.7 = (f32[768]{0:T(1024)S(1)}, f32[768]{0:T(1024)}, u32[]{:S(2)}) copy-start(f32[768]{0:T(1024)} %param.18) | copy-start | bytes 9220
  13.5 487.7 %all-to-all-start = ((bf16[32,256,512]{1,2,0:T(8,128)(2,1)}), bf16[32,256,512]{1,2,0:T(8,128)(2,1)}, u32[]{:S(2)}, u32[]{:S(2)}) async-start(bf16[32,256,512]{1,2,0:T(8,128)(2,1)} %tile.2), calls=%async_computation | async-start | bytes 16777216 | tf_op jit(solution)/shard_map/all_to_all | solution.py:15
  39.2 583.4 %all-gather.3.cloned.1.call-start = ((), (), s32[]{:S(2)}) async-start(), calls=%async_computation.4 | async-start | bytes 8650752 | tf_op jit(solution)/shard_map/all_gather | solution.py:154
  40.0 582.6 %all-gather.5.cloned.1.call-start = ((), (), s32[]{:S(2)}) async-start(), calls=%async_computation.5 | async-start | bytes 8650752 | tf_op jit(solution)/shard_map/all_gather | solution.py:160
  515.1 0.8 copy-start.2
  519.5 3.4 copy-start.1
  525.4 0.8 copy-start.2
  529.8 3.4 copy-start.1
  535.7 0.8 copy-start.2
  540.1 3.4 copy-start.1
  546.0 0.8 copy-start.2
  550.4 3.4 copy-start.1
  556.3 0.8 copy-start.2
  560.7 3.4 copy-start.1
  566.6 0.8 copy-start.2
  571.0 3.4 copy-start.1
  576.9 0.8 copy-start.2
  581.3 3.4 copy-start.1
  587.2 0.8 copy-start.2
  591.6 3.4 copy-start.1
  595.7 21.8 %copy-start.6 = (f32[2048]{0:T(1024)S(1)}, f32[2048]{0:T(1024)}, u32[]{:S(2)}) copy-start(f32[2048]{0:T(1024)} %param.23) | copy-start | bytes 24580
  597.2 19.0 %all-to-all-start.1 = ((bf16[4,64,2048]{2,1,0:T(8,128)(2,1)}), bf16[4,64,2048]{2,1,0:T(8,128)(2,1)S(1)}, u32[]{:S(2)}, u32[]{:S(2)}) async-start(bf16[4,64,2048]{2,1,0:T(8,128)(2,1)} %bitcast.4), calls=%async_computation.1 | async-start | bytes 2097152 | tf_op jit(solution)/shard_map/all_to_all | solution.py:27
  618.7 17.4 %all-to-all-start.2 = ((bf16[4,64,2048]{2,1,0:T(8,128)(2,1)}), bf16[4,64,2048]{2,1,0:T(8,128)(2,1)S(1)}, u32[]{:S(2)}, u32[]{:S(2)}) async-start(bf16[4,64,2048]{2,1,0:T(8,128)(2,1)} %broadcast_in_dim.17), calls=%async_computation.2 | async-start | bytes 2097152 | tf_op jit(solution)/shard_map/all_to_all | solution.py:33
Sparse Core Ops, SparseCore 0:
  41.8 249.9 all-gather.2
  293.6 203.0 all-gather.4
